TPU v7x, 768 devices: a whole 4x8x12 slice. The times are simulated.
768 devices in a mesh: ep: 48 (over z, x), tp: 16 (over y, core).
Axes of the slice: x: 4, y: 8, z: 12, core: 2. Of those that a mesh axis runs over, the one named last changes fastest.
Arguments:
- tokens: bfloat16 [1152, 3072], P('ep'), may hold values from -6 to 6
- norm_gain: float32 [3072], replicated, may hold values from 0.1 to 1.9
- routing: int32 [1152, 4], P('ep'), may hold values from 0 to 47, all different within a row; in each aligned block of 24 rows (0 to 23, 24 to 47, ...) at most 3 rows name the same one
- route_weight: float32 [1152, 4], P('ep'), may hold values from 0.05 to 1
- w_gate: bfloat16 [48, 3072, 3072], P('ep', None, 'tp'), may hold values from -0.3125 to 0.3125
- w_up: bfloat16 [48, 3072, 3072], P('ep', None, 'tp'), may hold values from -0.3125 to 0.3125
- w_down: bfloat16 [48, 3072, 3072], P('ep', 'tp'), may hold values from -0.01953125 to 0.01953125
Outputs:
- mixed: bfloat16 [1152, 3072], P('ep', 'tp')
Inputs may be any that keep to these rules, and one draw needn't show every extreme that they name: `routing`: each row names 4 different experts. Within the rows of one device (aligned blocks of 24 rows) no expert is named by more than 3 rows, a bound that some block reaches.
All inputs are finite; a program needn't handle non-finite values.
Results may differ from a plain program's by a relative error of at most 0.019.
Values may be sent and summed in bfloat16 or wider, within the bound.
A program may use at most 32 MiB of HBM per device.

v0:
```python
import jax
import jax.numpy as jnp
from jax import lax
from jax.sharding import PartitionSpec as P

NORM_EPS = 1e-06
CLAMP_LIMIT = 7.0
SIGMOID_SCALE = 1.702


def in_blocks(shard, dim, devices):
    shape = shard.shape
    parts = shard.reshape(*shape[:dim], devices, shape[dim] // devices, *shape[dim + 1 :])
    return jnp.moveaxis(parts, dim, 0)


def sum_at_owner(shard, axis, dim):
    parts = in_blocks(shard, dim, lax.axis_size(axis))
    arrived = lax.all_to_all(parts, axis, split_axis=0, concat_axis=0, tiled=True)
    return arrived.astype(jnp.float32).sum(axis=0)


def slot_index(route_rows, expert_total, capacity):
    flat_ids = route_rows.reshape(-1)
    one_hot = (flat_ids[:, None] == jnp.arange(expert_total, dtype=jnp.int32)[None, :]).astype(
        jnp.int32
    )
    before = jnp.cumsum(one_hot, axis=0) - one_hot
    ranked = jnp.sum(before * one_hot, axis=1)
    return flat_ids * capacity + ranked


def local(tokens, norm_gain, routing, route_weight, w_gate, w_up, w_down):
    tok_count = tokens.shape[0]
    width = tokens.shape[1]
    top_count = routing.shape[1]
    expert_total = lax.axis_size("ep") * w_gate.shape[0]
    capacity = max(2, tok_count * top_count // expert_total + 1)
    slice_width = width // lax.axis_size("tp")
    values = tokens.astype(jnp.float32)
    scaled = values * lax.rsqrt(jnp.mean(values * values, axis=-1, keepdims=True) + NORM_EPS)
    normal = (scaled * norm_gain).astype(jnp.bfloat16)
    dest = slot_index(routing, expert_total, capacity)
    slot_ids = jnp.arange(expert_total * capacity, dtype=jnp.int32)
    select = jnp.sum(dest.reshape(1, tok_count, top_count) == slot_ids[:, None, None], axis=2)
    sending = jnp.dot(
        select.astype(jnp.bfloat16), normal, preferred_element_type=jnp.float32
    ).astype(jnp.bfloat16)
    gate_mat = w_gate[0]
    up_mat = w_up[0]
    down_mat = w_down[0]
    own_share = lax.dynamic_slice_in_dim(
        sending, lax.axis_index("tp") * slice_width, slice_width, 1
    )
    arrived = lax.all_to_all(own_share, "ep", split_axis=0, concat_axis=0, tiled=True)
    pieces = lax.all_gather(arrived, "tp", axis=1, tiled=True)
    gate_pre = jnp.dot(pieces, gate_mat, preferred_element_type=jnp.float32)
    up_pre = jnp.dot(pieces, up_mat, preferred_element_type=jnp.float32)
    gated = jnp.minimum(gate_pre, CLAMP_LIMIT)
    upper = jnp.clip(up_pre, -CLAMP_LIMIT, CLAMP_LIMIT)
    hidden = ((upper + 1.0) * gated * jax.nn.sigmoid(SIGMOID_SCALE * gated)).astype(jnp.bfloat16)
    summed = sum_at_owner(
        lax.dot_general(
            down_mat, hidden, (((0,), (1,)), ((), ())), preferred_element_type=jnp.float32
        ).astype(jnp.bfloat16),
        "tp",
        0,
    )
    returned = summed.astype(jnp.bfloat16)
    back = lax.all_to_all(returned, "ep", split_axis=1, concat_axis=1, tiled=True)
    picked = back[:, dest].reshape(slice_width, tok_count, top_count)
    mixed = jnp.sum(picked.astype(jnp.float32) * route_weight[None, :, :], axis=2)
    return mixed.T.astype(jnp.bfloat16)


def solution(mesh):
    placed = (
        P("ep", None),
        P(),
        P("ep", None),
        P("ep", None),
        P("ep", None, "tp"),
        P("ep", None, "tp"),
        P("ep", "tp", None),
    )
    return jax.shard_map(
        local, mesh=mesh, in_specs=placed, out_specs=P("ep", "tp"), check_vma=False
    )
```

profile of v0, /device:TPU:1, one launch (start us, length us, event | category | flops | bytes accessed | tf_op | source)
XLA Modules:
  0.0 121.0 jit_solution(2651689145066277858)
XLA Ops:
  0.0 0.0 copy-start
  0.0 0.9 copy.20
  0.9 0.1 eq.28
  1.0 0.1 fusion.42
  1.0 0.1 reduce_window_sum.11
  1.2 0.2 select_reduce_fusion
  1.4 0.1 reduce_sum.53
  1.5 0.1 copy.22
  1.6 0.1 convert_reduce_fusion
  1.7 1.0 fusion.26
  2.7 1.4 %fusion.29 = bf16[144,3072]{1,0:T(8,128)(2,1)S(1)} fusion(bf16[24,3072]{1,0:T(8,128)(2,1)} %param.7, f32[3072]{0:T(1024)} %param.8, f32[24]{0:T(128)S(1)} %add_rsqrt_fusion, s32[144,24]{0,1:T(8,128)S(1)} %convert_reduce_fusion), kind=kOutput, calls=%fused_computation.19 | convolution fusion | flops 21532032 | bytes 1058400 | tf_op jit(solution)/shard_map/dot_general | solution.py:46
  4.1 0.1 dynamic-slice_convert_fusion
  4.2 30.0 %all_to_all.29 = bf16[48,3,192]{2,1,0:T(4,128)(2,1)S(1)} all-to-all(bf16[48,3,192]{2,1,0:T(4,128)(2,1)S(1)} %all_to_all.19), channel_id=1, replica_groups=mesh['ep'=48,'tp'=16] {'ep'}, dimensions={0} | all-to-all | bytes 110592 | tf_op jit(solution)/shard_map/all_to_all | solution.py:55
  34.3 0.1 all_to_all.21
  34.3 23.5 %all-gather = bf16[16,192,144]{1,2,0:T(8,128)(2,1)S(1)} all-gather(bf16[1,192,144]{1,2,0:T(8,128)(2,1)S(1)} %bitcast.51), channel_id=1, replica_groups=mesh['ep'=48,'tp'=16] {'tp'}, dimensions={0}, use_global_device_ids=true | all-gather | bytes 940032 | tf_op jit(solution)/shard_map/all_gather | solution.py:56
  57.8 0.4 copy.23
  58.2 1.2 %reshape.68 = bf16[3072,144]{0,1:T(8,128)(2,1)S(1)} reshape(bf16[16,192,144]{1,0,2:T(8,128)(2,1)S(1)} %copy.23) | data formatting | bytes 1769472
  59.5 1.8 %fusion.18 = f32[144,192]{1,0:T(8,128)S(1)} fusion(bf16[3072,144]{0,1:T(8,128)(2,1)S(1)} %reshape.68, bf16[1,3072,192]{1,2,0:T(8,128)(2,1)} %param.11), kind=kOutput, calls=%fused_computation.12 | convolution fusion | flops 169896960 | bytes 2174976 | tf_op jit(solution)/shard_map/dot_general | solution.py:57
  61.3 2.5 %fusion = bf16[3072,144]{0,1:T(8,128)(2,1)S(1)} fusion(bf16[1,192,3072]{2,1,0:T(8,128)(2,1)S(1)} %copy-done, f32[144,192]{1,0:T(8,128)S(1)} %fusion.18, bf16[3072,144]{0,1:T(8,128)(2,1)S(1)} %reshape.68, bf16[1,3072,192]{1,2,0:T(8,128)(2,1)} %param.12), kind=kOutput, calls=%fused_computation.2 | convolution fusion | flops 340429824 | bytes 4239360 | tf_op jit(solution)/shard_map/dot_general | solution.py:63
  63.8 1.3 %reshape.57 = bf16[16,192,144]{1,0,2:T(8,128)(2,1)S(1)} reshape(bf16[3072,144]{0,1:T(8,128)(2,1)S(1)} %fusion) | data formatting | bytes 1769472 | tf_op jit(solution)/shard_map/reshape | solution.py:13
  65.1 1.4 %copy.24 = bf16[16,192,144]{1,2,0:T(8,128)(2,1)} copy(bf16[16,192,144]{1,0,2:T(8,128)(2,1)S(1)} %reshape.57) | data formatting | bytes 1769472 | tf_op jit(solution)/shard_map/reshape | solution.py:13
  66.5 4.5 %all-to-all-start.1 = ((bf16[16,192,144]{1,2,0:T(8,128)(2,1)}), bf16[16,192,144]{1,2,0:T(8,128)(2,1)S(1)}, u32[]{:S(2)}, u32[]{:S(2)}) async-start(bf16[16,192,144]{1,2,0:T(8,128)(2,1)} %copy.24), calls=%async_computation.1 | async-start | bytes 2359296 | tf_op jit(solution)/shard_map/all_to_all | solution.py:19
  71.0 0.1 mul.76
  71.1 30.5 %all-to-all-done.1 = bf16[16,192,144]{1,2,0:T(8,128)(2,1)S(1)} async-done(((bf16[16,192,144]{1,2,0:T(8,128)(2,1)}), bf16[16,192,144]{1,2,0:T(8,128)(2,1)S(1)}, u32[]{:S(2)}, u32[]{:S(2)}) %all-to-all-start.1) | async-done | bytes 884768 | tf_op jit(solution)/shard_map/all_to_all | solution.py:19
  101.6 0.2 reduce_sum.56
  101.8 0.7 all_to_all.23
  102.5 4.5 %all-to-all-start.2 = ((bf16[192,48,3]{0,2,1:T(4,128)(2,1)}), bf16[192,48,3]{0,2,1:T(4,128)(2,1)S(1)}, u32[]{:S(2)}, u32[]{:S(2)}) async-start(bf16[192,48,3]{0,2,1:T(4,128)(2,1)} %all_to_all.23), calls=%async_computation.2 | async-start | bytes 196608 | tf_op jit(solution)/shard_map/all_to_all | solution.py:70
  107.0 0.1 copy.25
  107.1 12.2 %all-to-all-done.2 = bf16[192,48,3]{0,2,1:T(4,128)(2,1)S(1)} async-done(((bf16[192,48,3]{0,2,1:T(4,128)(2,1)}), bf16[192,48,3]{0,2,1:T(4,128)(2,1)S(1)}, u32[]{:S(2)}, u32[]{:S(2)}) %all-to-all-start.2) | async-done | bytes 55328 | tf_op jit(solution)/shard_map/all_to_all | solution.py:70
  119.4 0.1 all_to_all.25
  119.5 0.8 gather_fusion
  120.3 0.7 multiply_reduce_fusion
  (10 shorter events, 0.1 us)
Async XLA Ops:
  0.0 61.3 %copy-start = (bf16[1,192,3072]{2,1,0:T(8,128)(2,1)S(1)}, bf16[1,192,3072]{2,1,0:T(8,128)(2,1)}, u32[]{:S(2)}) copy-start(bf16[1,192,3072]{2,1,0:T(8,128)(2,1)} %param.13) | copy-start | bytes 3538948
  66.5 35.1 %all-to-all-start.1 = ((bf16[16,192,144]{1,2,0:T(8,128)(2,1)}), bf16[16,192,144]{1,2,0:T(8,128)(2,1)S(1)}, u32[]{:S(2)}, u32[]{:S(2)}) async-start(bf16[16,192,144]{1,2,0:T(8,128)(2,1)} %copy.24), calls=%async_computation.1 | async-start | bytes 2359296 | tf_op jit(solution)/shard_map/all_to_all | solution.py:19
  71.0 36.0 %copy-start.1 = (f32[24,4]{0,1:T(4,128)S(1)}, f32[24,4]{0,1:T(4,128)}, u32[]{:S(2)}) copy-start(f32[24,4]{0,1:T(4,128)} %param.10) | copy-start | bytes 1156
  102.5 16.9 %all-to-all-start.2 = ((bf16[192,48,3]{0,2,1:T(4,128)(2,1)}), bf16[192,48,3]{0,2,1:T(4,128)(2,1)S(1)}, u32[]{:S(2)}, u32[]{:S(2)}) async-start(bf16[192,48,3]{0,2,1:T(4,128)(2,1)} %all_to_all.23), calls=%async_computation.2 | async-start | bytes 196608 | tf_op jit(solution)/shard_map/all_to_all | solution.py:70
where the time goes:
time: 121 us
  blocking collectives  53.5 us (44%)
  waiting for transfers between devices  42.8 us (35%)
  starting transfers between devices  9 us (7%)
  local copies, waits for them, and re-layouts  7.38 us (6%)
  matrix products  5.73 us (5%)
  other arithmetic  2.5 us (2%)
    all_to_all x1, waiting for transfers between devices, sum_at_owner(): lax.all_to_all(parts, axis, split_axis=0, concat_axis=0, tiled=True)  30.5 us
    all_to_all x1, blocking collectives, local(): lax.all_to_all(own_share, 'ep', split_axis=0, concat_axis=0, tiled=True)  30 us
    all_gather x1, blocking collectives, local(): pieces = lax.all_gather(arrived, 'tp', axis=1, tiled=True)  23.5 us
    all_to_all x1, waiting for transfers between devices, local(): lax.all_to_all(returned, 'ep', split_axis=1, concat_axis=1, tiled=True)  12.2 us
    all_to_all x1, starting transfers between devices, local(): lax.all_to_all(returned, 'ep', split_axis=1, concat_axis=1, tiled=True)  4.52 us
    all_to_all x1, starting transfers between devices, sum_at_owner(): lax.all_to_all(parts, axis, split_axis=0, concat_axis=0, tiled=True)  4.47 us
    reshape x2, local copies, waits for them, and re-layouts, in_blocks(): shard.reshape(*shape[:dim], devices, shape[dim] // devices, *shape[dim +...  2.68 us
    dot_general x1, matrix products, local(): lax.dot_general(down_mat, hidden, (((0,), (1,)), ((), ())), preferred_ele...  2.54 us
  transfers between devices with their start and end apart: 2, of which 2 were waited for; matrix products, arithmetic and copies ran while one was open for 0% of the time, Pallas kernels for 0%

commit v1 on v0

v1 whole, which is shorter than its diff:
```python
import functools

import jax
import jax.numpy as jnp
from jax import lax
from jax.experimental import pallas as pl
from jax.experimental.pallas import tpu as pltpu
from jax.sharding import PartitionSpec as P

NORM_EPS = 1e-06
CLAMP_LIMIT = 7.0
SIGMOID_SCALE = 1.702
MESH = pl.DeviceIdType.MESH
NX = 4
CHUNKS = 3
SHARES = 4
F32 = jnp.float32
BF16 = jnp.bfloat16


def dot(a, b):
    return jnp.dot(a, b, preferred_element_type=F32)


def kernel(
    nz, ny, tok_ref, gain_ref, route_ref, rw_ref, wg_ref, wu_ref, wd_ref, out_ref,
    gw, uw, dw, sbuf, rbuf, xs, ls, lr, ss, sr, rsend, rret, msend, mrecv,
    w_sem, wp_send, wp_recv, d_send, d_recv, y_send, y_recv,
    l_send, l_recv, s_send, s_recv, r_send, r_recv, m_send, m_recv,
):
    ep, tp = lax.axis_index("ep"), lax.axis_index("tp")
    z, x = lax.div(ep, NX), lax.rem(ep, NX)
    y, core = lax.div(tp, 2), lax.rem(tp, 2)
    other = 1 - core
    toks = tok_ref.shape[0]
    peers = sbuf.shape[0]
    per = peers // CHUNKS
    half = sbuf.shape[2]
    share = 2 * half
    window = rsend.shape[2]
    lanes = out_ref.shape[1]

    def dev(dz, dx, dy, at):
        return (
            lax.rem(z + dz + nz, nz) * NX + lax.rem(x + dx + NX, NX),
            lax.rem(y + dy + ny, ny) * 2 + at,
        )

    def far(i):
        return (i + 1) // 2 if i % 2 else (nz - i // 2) % nz

    def remote(src, dst, send, recv, to):
        return pltpu.make_async_remote_copy(
            src_ref=src, dst_ref=dst, send_sem=send, recv_sem=recv, device_id=to, device_id_type=MESH
        )

    partner = dev(0, 0, 0, other)
    sources = [dev(-far(j // 2), -(2 * (j % 2) + other), 0, other) for j in range(peers)]
    targets = [dev(far(j // 2), 2 * (j % 2) + core, 0, other) for j in range(peers)]

    barrier = pltpu.get_barrier_semaphore()
    for to in sources[::-1] + [dev(0, 0, dy, core) for dy in (2, -2, 1, -1)] + [partner]:
        pl.semaphore_signal(barrier, inc=1, device_id=to, device_id_type=MESH)

    local = [
        pltpu.make_async_copy(wg_ref, gw.at[0], w_sem.at[0]),
        pltpu.make_async_copy(wu_ref, uw.at[0], w_sem.at[1]),
    ]
    for copy in local:
        copy.start()
    out_width = dw.shape[3]
    for q in range(ny):
        pltpu.make_async_copy(
            wd_ref.at[:, pl.ds(q * out_width, out_width)], dw.at[0, q], w_sem.at[2]
        ).start()

    values = tok_ref[...].astype(F32)
    scale = lax.rsqrt(jnp.mean(values * values, axis=-1, keepdims=True) + NORM_EPS)
    at = pl.multiple_of(lax.rem(y, SHARES) * share, 128)
    shared = tok_ref[:, pl.ds(at, share)].astype(F32)
    normal = (shared * scale * gain_ref[:, pl.ds(at, share)]).astype(BF16)

    row = lax.broadcasted_iota(jnp.int32, (peers * 8, 1), 0)
    order = row >> 4
    dz = jnp.where((order & 1) == 1, (order + 1) >> 1, jnp.where(order == 0, 0, nz - (order >> 1)))
    ez = z + dz
    ez = jnp.where(ez >= nz, ez - nz, ez)
    ex = (x + 2 * ((row >> 3) & 1) + core) & (NX - 1)
    expert = ez * NX + ex
    in_half, place = (row >> 2) & 1, row & 3
    routes, weights = route_ref[...], rw_ref[...]
    hit = jnp.zeros((peers * 8, toks), F32)
    weight = jnp.zeros((peers * 8, toks), F32)
    for k in range(routes.shape[0]):
        same = routes[k : k + 1] == expert
        hit = hit + jnp.where(same, 1.0, 0.0)
        weight = weight + jnp.where(same, weights[k : k + 1], 0.0)
    earlier = jnp.where(
        lax.broadcasted_iota(jnp.int32, (toks, toks), 0) < lax.broadcasted_iota(jnp.int32, (toks, toks), 1),
        1.0,
        0.0,
    ).astype(BF16)
    before = dot(hit.astype(BF16), earlier)
    here = jnp.where(before == place.astype(F32), hit, 0.0)
    here_0 = jnp.where(in_half == 0, here, 0.0)
    here_1 = here - here_0
    sending = dot(here_0.astype(BF16), normal[:, :half]) + dot(here_1.astype(BF16), normal[:, half:])
    sbuf[...] = sending.reshape(peers, 8, half).astype(BF16)
    mixing = []
    for picks in (here_0, here_1):
        exact = (picks * weight).T
        high = exact.astype(BF16)
        mixing += [high, (exact - high.astype(F32)).astype(BF16)]

    pl.semaphore_wait(barrier, peers + 5)
    for j in reversed(range(peers)):
        remote(sbuf.at[j], rbuf.at[j], d_send, d_recv.at[j // per], targets[j]).start()

    for copy in local:
        copy.wait()
    pltpu.make_async_copy(dw.at[0], dw.at[0], w_sem.at[2]).wait()
    pushes = [
        remote(buf.at[0], buf.at[1], wp_send.at[n], wp_recv.at[n], partner)
        for n, buf in enumerate((gw, uw, dw))
    ]
    for push in pushes:
        push.start()

    rows = per * 3
    compact_row = lax.broadcasted_iota(jnp.int32, (rows, per * 8), 0)
    compact_col = lax.broadcasted_iota(jnp.int32, (rows, per * 8), 1)
    third = (compact_row * 11) >> 5
    meets = ((compact_col >> 3) == third) & ((compact_col & 3) == compact_row - 3 * third)
    first = jnp.where(meets & ((compact_col & 4) == 0), 1.0, 0.0)
    second = jnp.where(meets & ((compact_col & 4) == 4), 1.0, 0.0)
    first_c, second_c = first.astype(BF16), second.astype(BF16)
    first_e, second_e = first.T.astype(BF16), second.T.astype(BF16)

    for k in range(CHUNKS):
        part = rbuf.at[pl.ds(k * per, per)]
        remote(part, part, d_send, d_recv.at[k], partner).wait_recv()
        got = part[...].astype(F32).reshape(per * 8, half).astype(BF16)
        span = pl.ds(k * rows, rows)
        xs[0, span, :half] = dot(first_c, got).astype(BF16)
        xs[0, span, half:] = dot(second_c, got).astype(BF16)
        whole = xs.at[0, span]
        left, right = xs.at[0, span, pl.ds(0, half)], xs.at[0, span, pl.ds(half, half)]
        remote(left, xs.at[3, span, pl.ds(0, half)], y_send, y_recv.at[2], dev(0, 0, 2, core)).start()
        remote(right, xs.at[3, span, pl.ds(half, half)], y_send, y_recv.at[2], dev(0, 0, -2, core)).start()
        remote(whole, xs.at[1, span], y_send, y_recv.at[0], dev(0, 0, 1, core)).start()
        remote(whole, xs.at[2, span], y_send, y_recv.at[1], dev(0, 0, -1, core)).start()

    for push in pushes[:2]:
        push.wait_recv()
    sums = None
    for n, dy in enumerate((0, -1, 1, 2)):
        if n:
            remote(xs.at[n], xs.at[n], y_send, y_recv.at[n - 1], partner).wait_recv()
        at_share = lax.rem(y + dy + SHARES, SHARES)
        block = xs[n]
        span = pl.ds(pl.multiple_of(at_share * share, 128), share)
        terms = [
            lax.dot_general(block, w[side, :, span], (((1,), (1,)), ((), ())), preferred_element_type=F32)
            for side in range(2)
            for w in (gw, uw)
        ]
        sums = terms if sums is None else [a + b for a, b in zip(sums, terms)]
    hidden = []
    for side in range(2):
        gated = jnp.minimum(sums[2 * side], CLAMP_LIMIT)
        upper = jnp.clip(sums[2 * side + 1], -CLAMP_LIMIT, CLAMP_LIMIT)
        hidden.append(((upper + 1.0) * gated * jax.nn.sigmoid(SIGMOID_SCALE * gated)).astype(BF16))

    pushes[2].wait_recv()
    sign = 1 - 2 * core

    def partial_for(steps):
        to = lax.rem(y + steps * sign + ny, ny)
        return dot(hidden[0], dw[0, to]) + dot(hidden[1], dw[1, to])

    long, short = ny // 2, ny // 2 - 1
    ahead, behind = dev(0, 0, sign, core), dev(0, 0, -sign, core)
    backwards = list(reversed(range(CHUNKS)))
    for step in range(long):
        term = partial_for(long - step)
        for k in backwards:
            piece = term[k * rows : (k + 1) * rows]
            if step:
                got = lr.at[step - 1, k]
                remote(got, got, l_send, l_recv.at[step - 1, k], partner).wait_recv()
                piece = piece + got[...].astype(F32)
            ls[step, k] = piece.astype(BF16)
            remote(ls.at[step, k], lr.at[step, k], l_send, l_recv.at[step, k], ahead).start()
        if step < short:
            term = partial_for(step - short)
            for k in backwards:
                piece = term[k * rows : (k + 1) * rows]
                if step:
                    got = sr.at[step - 1, k]
                    remote(got, got, s_send, s_recv.at[step - 1, k], partner).wait_recv()
                    piece = piece + got[...].astype(F32)
                ss[step, k] = piece.astype(BF16)
                remote(ss.at[step, k], sr.at[step, k], s_send, s_recv.at[step, k], behind).start()
    term = partial_for(0)
    for k in backwards:
        got_s, got_l = sr.at[short - 1, k], lr.at[long - 1, k]
        remote(got_s, got_s, s_send, s_recv.at[short - 1, k], partner).wait_recv()
        remote(got_l, got_l, l_send, l_recv.at[long - 1, k], partner).wait_recv()
        total = term[k * rows : (k + 1) * rows] + got_s[...].astype(F32) + got_l[...].astype(F32)
        total = total.astype(BF16)
        spread = dot(first_e, total[:, :window]) + dot(second_e, total[:, out_width - window :])
        rsend[pl.ds(k * per, per)] = spread.reshape(per, 8, window).astype(BF16)
        for j in reversed(range(k * per, (k + 1) * per)):
            remote(rsend.at[j], rret.at[j], r_send, r_recv, sources[j]).start()

    remote(rret, rret, r_send, r_recv, partner).wait_recv()
    back = rret[...].astype(F32).reshape(peers * 8, window).astype(BF16)
    part_0 = dot(mixing[0], back) + dot(mixing[1], back)
    part_1 = dot(mixing[2], back) + dot(mixing[3], back)
    is_0 = core == 0
    msend[...] = jnp.where(is_0, part_1, part_0)
    swap = remote(msend, mrecv, m_send, m_recv, partner)
    swap.start()
    own = jnp.where(is_0, part_0, part_1)
    swap.wait_recv()
    full = own + mrecv[...]
    out_ref[...] = jnp.where(is_0, full[:, :lanes], full[:, window - lanes :]).astype(BF16)

    remote(sbuf, rbuf, d_send, m_recv, partner).wait_send()
    for push in pushes:
        push.wait_send()
    others = xs.at[pl.ds(1, 3)]
    remote(others, others, y_send, m_recv, partner).wait_send()
    remote(ls, lr, l_send, m_recv, partner).wait_send()
    remote(ss, sr, s_send, m_recv, partner).wait_send()
    remote(rsend, rret, r_send, m_recv, partner).wait_send()
    swap.wait_send()


def local(nz, ny, tokens, norm_gain, routing, route_weight, w_gate, w_up, w_down):
    toks, width = tokens.shape
    depth = w_gate.shape[2]
    peers = nz * NX // 2
    per = peers // CHUNKS
    rows = per * 3
    share = width // SHARES
    half = share // 2
    out_width = width // ny
    window = 256
    vmem = functools.partial(pl.BlockSpec, memory_space=pltpu.VMEM)
    hbm = functools.partial(pl.BlockSpec, memory_space=pl.ANY)
    dma = pltpu.SemaphoreType.DMA
    long, short = ny // 2, ny // 2 - 1
    return pl.pallas_call(
        functools.partial(kernel, nz, ny),
        out_shape=jax.ShapeDtypeStruct((toks, width // (2 * ny)), BF16),
        in_specs=[vmem()] * 4 + [hbm()] * 3,
        out_specs=vmem(),
        scratch_shapes=[
            pltpu.VMEM((2, depth, width), BF16),
            pltpu.VMEM((2, depth, width), BF16),
            pltpu.VMEM((2, ny, depth, out_width), BF16),
            pltpu.VMEM((peers, 8, half), BF16),
            pltpu.VMEM((peers, 8, half), BF16),
            pltpu.VMEM((SHARES, CHUNKS * rows, share), BF16),
            pltpu.VMEM((long, CHUNKS, rows, out_width), BF16),
            pltpu.VMEM((long, CHUNKS, rows, out_width), BF16),
            pltpu.VMEM((short, CHUNKS, rows, out_width), BF16),
            pltpu.VMEM((short, CHUNKS, rows, out_width), BF16),
            pltpu.VMEM((peers, 8, window), BF16),
            pltpu.VMEM((peers, 8, window), BF16),
            pltpu.VMEM((toks, window), F32),
            pltpu.VMEM((toks, window), F32),
            dma((3,)),
            dma((3,)),
            dma((3,)),
            dma,
            dma((CHUNKS,)),
            dma,
            dma((3,)),
            dma,
            dma((long, CHUNKS)),
            dma,
            dma((short, CHUNKS)),
            dma,
            dma,
            dma,
            dma,
        ],
        compiler_params=pltpu.CompilerParams(collective_id=0, has_side_effects=True),
    )(
        tokens,
        norm_gain.reshape(1, width),
        routing.T,
        route_weight.T,
        w_gate[0].T,
        w_up[0].T,
        w_down.reshape(depth, width),
    )


def solution(mesh):
    placed = (
        P("ep", None),
        P(),
        P("ep", None),
        P("ep", None),
        P("ep", None, "tp"),
        P("ep", None, "tp"),
        P("ep", "tp", None),
    )
    body = functools.partial(local, mesh.shape["ep"] // NX, mesh.shape["tp"] // 2)
    return jax.shard_map(body, mesh=mesh, in_specs=placed, out_specs=P("ep", "tp"), check_vma=False)
```

time: 121 us -> 60.4 us (0.50)
  Pallas kernels: 0 us -> 58.9 us
  blocking collectives: 53.5 us -> 0 us
  waiting for transfers between devices: 42.8 us -> 0 us
  starting transfers between devices: 9 us -> 0 us
  local copies, waits for them, and re-layouts: 7.38 us -> 1.31 us
  matrix products: 5.73 us -> 0 us
  other arithmetic: 2.5 us -> 0 us
    pallas_call x0 -> x1, Pallas kernels: none -> 58.9 us  [local(): pl.pallas_call(functools.partial(kernel, nz, ny), out_shape=jax.ShapeDtyp...]
    all_to_all x2 -> x0, waiting for transfers between devices: 42.8 us -> none  [the longest x1 30.5 us: sum_at_owner(): lax.all_to_all(parts, axis, split_axis=0, concat_axis=0, tiled=True)]
    all_to_all x1 -> x0, blocking collectives: 30 us -> none  [local(): lax.all_to_all(own_share, 'ep', split_axis=0, concat_axis=0, tiled=True)]
    all_gather x1 -> x0, blocking collectives: 23.5 us -> none  [local(): pieces = lax.all_gather(arrived, 'tp', axis=1, tiled=True)]
    all_to_all x2 -> x0, starting transfers between devices: 9 us -> none  [the longest x1 4.52 us: local(): lax.all_to_all(returned, 'ep', split_axis=1, concat_axis=1, tiled=True)]
    dot_general x3 -> x0, matrix products: 5.73 us -> none  [the longest x1 2.54 us: local(): lax.dot_general(down_mat, hidden, (((0,), (1,)), ((), ())), preferred_ele...]
    reshape x2 -> x0, local copies, waits for them, and re-layouts: 2.68 us -> none  [in_blocks(): shard.reshape(*shape[:dim], devices, shape[dim] // devices, *shape[dim +...]
    reduce_sum x5 -> x0, other arithmetic: 2.25 us -> none  [the longest x1 1.05 us: local(): jnp.mean(values * values, axis=-1, keepdims=True) + NORM_EPS]
  transfers between devices with their start and end apart: 2 -> 0, of which waited for: 2 -> 0; matrix products, arithmetic and copies ran while one was open for 0% -> 0% of each run, Pallas kernels for 0% -> 0%
where the time goes in v1:
time: 60.4 us; the launch traced here: 60.2 us
  Pallas kernels  58.9 us (98%)
  local copies, waits for them, and re-layouts  1.31 us (2%)
    pallas_call x1, Pallas kernels, local(): pl.pallas_call(functools.partial(kernel, nz, ny), out_shape=jax.ShapeDtyp...  58.9 us
    unnamed x1, local copies, waits for them, and re-layouts  1.31 us

profile of v1, /device:TPU:1, one launch (start us, length us, event | category | flops | bytes accessed | tf_op | source)
XLA Modules:
  0.0 60.2 jit_solution(1755430817201502435)
XLA Ops:
  0.0 58.9 %shard_map.73 = bf16[24,192]{1,0:T(8,128)(2,1)} custom-call(bf16[24,3072]{1,0:T(8,128)(2,1)} %tok_ref.1, f32[1,3072]{1,0:T(1,128)} %bitcast.13, s32[4,24]{1,0:T(4,128)} %bitcast.14, f32[4,24]{1,0:T(4,128)} %bitcast.15, bf16[192,3072]{1,0:T(8,128)(2,1)} %bitcast.10, bf16[192,3072]{1,0:T(8,128)(2,1)} %bitcast.11, bf16[192,3072]{1,0:T(8,128)(2,1)} %bitcast.12), custom_call_target="tpu_custom_call" | custom-call | tf_op jit(solution)/shard_map/pallas_call | solution.py:254
  58.9 1.3 %copy.9 = bf16[24,192]{1,0:T(8,128)(2,1)} copy(bf16[24,192]{1,0:T(8,128)(2,1)} %shard_map.73) | data formatting | bytes 18432

commit v2 on v1

v2 whole, which is shorter than its diff:
```python
import functools

import jax
import jax.numpy as jnp
from jax import lax
from jax.experimental import pallas as pl
from jax.experimental.pallas import tpu as pltpu
from jax.sharding import PartitionSpec as P

NORM_EPS = 1e-06
CLAMP_LIMIT = 7.0
SIGMOID_SCALE = 1.702
MESH = pl.DeviceIdType.MESH
NX = 4
CHUNKS = 3
SHARES = 4
F32 = jnp.float32
BF16 = jnp.bfloat16


def dot(a, b):
    return jnp.dot(a, b, preferred_element_type=F32)


def kernel(
    nz, ny, tok_ref, gain_ref, route_ref, rw_ref, wg_ref, wu_ref, wd_ref, out_ref,
    gw, uw, dw, sbuf, rbuf, xs, ssend, srecv, rsend, rret,
    w_sem, wp_send, wp_recv, d_send, d_recv, y_send, y_recv, s_send, s_recv, r_send, r_recv,
):
    ep, tp = lax.axis_index("ep"), lax.axis_index("tp")
    z, x = lax.div(ep, NX), lax.rem(ep, NX)
    y, core = lax.div(tp, 2), lax.rem(tp, 2)
    other = 1 - core
    toks = tok_ref.shape[0]
    peers = sbuf.shape[0]
    per = peers // CHUNKS
    half = sbuf.shape[2]
    share = 2 * half
    lanes = out_ref.shape[1]

    def dev(dz, dx, dy, at):
        return (
            lax.rem(z + dz + nz, nz) * NX + lax.rem(x + dx + NX, NX),
            lax.rem(y + dy + ny, ny) * 2 + at,
        )

    def far(i):
        return (i + 1) // 2 if i % 2 else (nz - i // 2) % nz

    def remote(src, dst, send, recv, to):
        return pltpu.make_async_remote_copy(
            src_ref=src, dst_ref=dst, send_sem=send, recv_sem=recv, device_id=to, device_id_type=MESH
        )

    partner = dev(0, 0, 0, other)
    def source(j, at):
        return dev(-far(j // 2), -(2 * (j % 2) + other), 0, at)

    sources = [source(j, other) for j in range(peers)]
    targets = [dev(far(j // 2), 2 * (j % 2) + core, 0, other) for j in range(peers)]

    barrier = pltpu.get_barrier_semaphore()
    for to in sources[::-1] + [dev(0, 0, dy, core) for dy in (2, -2, 1, -1)] + [partner]:
        pl.semaphore_signal(barrier, inc=1, device_id=to, device_id_type=MESH)

    local = [
        pltpu.make_async_copy(wg_ref, gw.at[0], w_sem.at[0]),
        pltpu.make_async_copy(wu_ref, uw.at[0], w_sem.at[1]),
    ]
    for copy in local:
        copy.start()
    out_width = dw.shape[3]
    for q in range(ny):
        pltpu.make_async_copy(
            wd_ref.at[:, pl.ds(q * out_width, out_width)], dw.at[0, q], w_sem.at[2]
        ).start()

    values = tok_ref[...].astype(F32)
    scale = lax.rsqrt(jnp.mean(values * values, axis=-1, keepdims=True) + NORM_EPS)
    at = pl.multiple_of(lax.rem(y, SHARES) * share, 128)
    shared = tok_ref[:, pl.ds(at, share)].astype(F32)
    normal = (shared * scale * gain_ref[:, pl.ds(at, share)]).astype(BF16)

    routes, weights = route_ref[...], rw_ref[...]
    earlier = jnp.where(
        lax.broadcasted_iota(jnp.int32, (toks, toks), 0) < lax.broadcasted_iota(jnp.int32, (toks, toks), 1),
        1.0,
        0.0,
    ).astype(BF16)

    def placed(parity):
        row = lax.broadcasted_iota(jnp.int32, (peers * 8, 1), 0)
        order = row >> 4
        dz = jnp.where((order & 1) == 1, (order + 1) >> 1, jnp.where(order == 0, 0, nz - (order >> 1)))
        ez = z + dz
        ez = jnp.where(ez >= nz, ez - nz, ez)
        expert = ez * NX + ((x + 2 * ((row >> 3) & 1) + parity) & (NX - 1))
        hit = jnp.zeros((peers * 8, toks), F32)
        weight = jnp.zeros((peers * 8, toks), F32)
        for k in range(routes.shape[0]):
            same = routes[k : k + 1] == expert
            hit = hit + jnp.where(same, 1.0, 0.0)
            weight = weight + jnp.where(same, weights[k : k + 1], 0.0)
        before = dot(hit.astype(BF16), earlier)
        here = jnp.where(before == (row & 3).astype(F32), hit, 0.0)
        return here, weight, (row >> 2) & 1

    here, _, in_half = placed(core)
    here_0 = jnp.where(in_half == 0, here, 0.0)
    here_1 = here - here_0
    sending = dot(here_0.astype(BF16), normal[:, :half]) + dot(here_1.astype(BF16), normal[:, half:])
    sbuf[...] = sending.reshape(peers, 8, half).astype(BF16)

    pl.semaphore_wait(barrier, peers + 5)
    for j in reversed(range(peers)):
        remote(sbuf.at[j], rbuf.at[j], d_send, d_recv.at[j // per], targets[j]).start()

    for copy in local:
        copy.wait()
    pltpu.make_async_copy(dw.at[0], dw.at[0], w_sem.at[2]).wait()
    pushes = [
        remote(buf.at[0], buf.at[1], wp_send.at[n], wp_recv.at[n], partner)
        for n, buf in enumerate((gw, uw, dw))
    ]
    for push in pushes:
        push.start()

    rows = per * 3
    compact_row = lax.broadcasted_iota(jnp.int32, (rows, per * 8), 0)
    compact_col = lax.broadcasted_iota(jnp.int32, (rows, per * 8), 1)
    third = (compact_row * 11) >> 5
    meets = ((compact_col >> 3) == third) & ((compact_col & 3) == compact_row - 3 * third)
    first = jnp.where(meets & ((compact_col & 4) == 0), 1.0, 0.0)
    second = jnp.where(meets & ((compact_col & 4) == 4), 1.0, 0.0)
    first_c, second_c = first.astype(BF16), second.astype(BF16)
    first_e, second_e = first.T.astype(BF16), second.T.astype(BF16)

    summed = []
    for sender in range(2):
        here, weight, _ = placed(1 - sender)
        summed.append(here * weight)
    exact = jnp.concatenate(summed, axis=0).T
    lane_half = (lax.broadcasted_iota(jnp.int32, exact.shape, 1) >> 2) & 1
    mixing = []
    for part in range(2):
        kept = jnp.where(lane_half == part, exact, 0.0)
        high = kept.astype(BF16)
        mixing += [high, (kept - high.astype(F32)).astype(BF16)]
    mixing = jnp.concatenate(mixing, axis=0)

    far_rows, near_rows = (2,), (0, 1)
    groups = (far_rows, near_rows)
    spans = [pl.ds(g[0] * rows, len(g) * rows) for g in groups]
    for k in (0, 2, 1):
        part = rbuf.at[pl.ds(k * per, per)]
        remote(part, part, d_send, d_recv.at[k], partner).wait_recv()
        got = part[...].astype(F32).reshape(per * 8, half).astype(BF16)
        span = pl.ds(k * rows, rows)
        xs[0, span, :half] = dot(first_c, got).astype(BF16)
        xs[0, span, half:] = dot(second_c, got).astype(BF16)
        g = 0 if k in far_rows else 1
        whole = xs.at[0, span]
        left, right = xs.at[0, span, pl.ds(0, half)], xs.at[0, span, pl.ds(half, half)]
        remote(left, xs.at[3, span, pl.ds(0, half)], y_send, y_recv.at[2, g], dev(0, 0, 2, core)).start()
        remote(right, xs.at[3, span, pl.ds(half, half)], y_send, y_recv.at[2, g], dev(0, 0, -2, core)).start()
        remote(whole, xs.at[1, span], y_send, y_recv.at[0, g], dev(0, 0, 1, core)).start()
        remote(whole, xs.at[2, span], y_send, y_recv.at[1, g], dev(0, 0, -1, core)).start()

    for push in pushes:
        push.wait_recv()

    def hidden_of(g):
        sums = None
        for n, dy in enumerate((0, -1, 1, 2)):
            if n:
                part = xs.at[n, spans[g]]
                remote(part, part, y_send, y_recv.at[n - 1, g], partner).wait_recv()
            block = xs[n, spans[g]]
            span = pl.ds(pl.multiple_of(lax.rem(y + dy + SHARES, SHARES) * share, 128), share)
            terms = [
                lax.dot_general(block, w[side, :, span], (((1,), (1,)), ((), ())), preferred_element_type=F32)
                for side in range(2)
                for w in (gw, uw)
            ]
            sums = terms if sums is None else [a + b for a, b in zip(sums, terms)]
        hidden = []
        for side in range(2):
            gated = jnp.minimum(sums[2 * side], CLAMP_LIMIT)
            upper = jnp.clip(sums[2 * side + 1], -CLAMP_LIMIT, CLAMP_LIMIT)
            hidden.append(((upper + 1.0) * gated * jax.nn.sigmoid(SIGMOID_SCALE * gated)).astype(BF16))
        return hidden

    sign = 1 - 2 * core
    ahead, ahead2 = dev(0, 0, sign, core), dev(0, 0, 2 * sign, core)
    behind, behind2 = dev(0, 0, -sign, core), dev(0, 0, -2 * sign, core)

    def term(hidden, steps):
        to = lax.rem(y + steps * sign + ny, ny)
        return dot(hidden[0], dw[0, to]) + dot(hidden[1], dw[1, to])

    def ship(slot, g, value, to):
        ssend[slot, spans[g]] = value.astype(BF16)
        remote(
            ssend.at[slot, spans[g]], srecv.at[slot, spans[g]], s_send, s_recv.at[slot, g], to
        ).start()

    def take(slot, g):
        part = srecv.at[slot, spans[g]]
        remote(part, part, s_send, s_recv.at[slot, g], partner).wait_recv()
        return part[...].astype(F32)

    def first_stage(g, hidden):
        ship(0, g, term(hidden, 4), ahead2)
        ship(1, g, term(hidden, 3), ahead)
        ship(2, g, term(hidden, -3), behind)
        ship(3, g, term(hidden, 1), ahead)
        ship(4, g, term(hidden, -1), behind)

    def relay(g, hidden):
        own, own_s = term(hidden, 2), term(hidden, -2)
        ship(5, g, own + take(0, g) + take(1, g), ahead2)
        ship(6, g, own_s + take(2, g), behind2)

    is_0 = core == 0
    lane = 128

    def give_back(g, hidden):
        total = term(hidden, 0)
        for slot in (3, 4, 6, 5):
            total = total + take(slot, g)
        total = total.astype(BF16)
        for k in reversed(groups[g]):
            at = (k - groups[g][0]) * rows
            piece = total[at : at + rows]
            ends, middle = dot(first_e, piece), dot(second_e, piece[:, lane : 2 * lane])
            spread_0, spread_1 = ends[:, :lane] + middle, ends[:, 2 * lane :] + middle
            span = pl.ds(k * per, per)
            same = jnp.where(is_0, spread_0, spread_1).reshape(per, 8, lane).astype(BF16)
            cross = jnp.where(is_0, spread_1, spread_0).reshape(per, 8, lane).astype(BF16)
            rsend[0, span] = same
            rsend[1, span] = cross
            for j in reversed(range(k * per, (k + 1) * per)):
                remote(rsend.at[1, j], rret.at[core, j], r_send.at[1], r_recv.at[1, g], source(j, other)).start()
                if j:
                    remote(rsend.at[0, j], rret.at[core, j], r_send.at[0], r_recv.at[0, g], source(j, core)).start()
                    continue

                @pl.when(is_0)
                def _():
                    remote(rsend.at[0, 0], rret.at[core, 0], r_send.at[2], r_recv.at[0, 2], source(0, core)).start()

                @pl.when(core == 1)
                def _():
                    rret[1, 0] = same[0]

    hidden_far = hidden_of(0)
    first_stage(0, hidden_far)
    hidden_near = hidden_of(1)
    relay(0, hidden_far)
    first_stage(1, hidden_near)
    give_back(0, hidden_far)
    relay(1, hidden_near)
    give_back(1, hidden_near)

    for g in range(2):
        begin, count = groups[g][0] * per, len(groups[g]) * per
        crossed = rret.at[other, pl.ds(begin, count)]
        remote(crossed, crossed, d_send, r_recv.at[1, g], partner).wait_recv()
        skipped = 0 if begin else 1
        stayed = rret.at[core, pl.ds(begin + skipped, count - skipped)]
        remote(stayed, stayed, d_send, r_recv.at[0, g], partner).wait_recv()

    own_chip = remote(rsend.at[0, 0], rret.at[core, 0], r_send.at[2], r_recv.at[0, 2], partner)

    @pl.when(is_0)
    def _():
        own_chip.wait_recv()

    back = rret[...].astype(F32).reshape(2 * peers * 8, lane).astype(BF16)
    mixed = dot(mixing, back)
    ends = mixed[:toks] + mixed[toks : 2 * toks]
    middle = mixed[2 * toks : 3 * toks] + mixed[3 * toks :]
    out_0 = jnp.concatenate([ends, middle[:, : lanes - lane]], axis=1)
    out_1 = jnp.concatenate([middle[:, 2 * lane - lanes :], ends], axis=1)
    out_ref[...] = jnp.where(is_0, out_0, out_1).astype(BF16)

    remote(sbuf, rbuf, d_send, d_recv.at[0], partner).wait_send()
    for push in pushes:
        push.wait_send()
    others = xs.at[pl.ds(1, 3)]
    remote(others, others, y_send, d_recv.at[0], partner).wait_send()
    remote(ssend, srecv, s_send, d_recv.at[0], partner).wait_send()
    remote(rsend.at[1], rret.at[0], r_send.at[1], d_recv.at[0], partner).wait_send()
    stayed = rsend.at[0, pl.ds(1, peers - 1)]
    remote(stayed, stayed, r_send.at[0], d_recv.at[0], partner).wait_send()

    @pl.when(is_0)
    def _():
        own_chip.wait_send()


def local(nz, ny, tokens, norm_gain, routing, route_weight, w_gate, w_up, w_down):
    toks, width = tokens.shape
    depth = w_gate.shape[2]
    peers = nz * NX // 2
    per = peers // CHUNKS
    rows = per * 3
    share = width // SHARES
    half = share // 2
    out_width = width // ny
    vmem = functools.partial(pl.BlockSpec, memory_space=pltpu.VMEM)
    hbm = functools.partial(pl.BlockSpec, memory_space=pl.ANY)
    dma = pltpu.SemaphoreType.DMA
    return pl.pallas_call(
        functools.partial(kernel, nz, ny),
        out_shape=jax.ShapeDtypeStruct((toks, width // (2 * ny)), BF16),
        in_specs=[vmem()] * 4 + [hbm()] * 3,
        out_specs=vmem(),
        scratch_shapes=[
            pltpu.VMEM((2, depth, width), BF16),
            pltpu.VMEM((2, depth, width), BF16),
            pltpu.VMEM((2, ny, depth, out_width), BF16),
            pltpu.VMEM((peers, 8, half), BF16),
            pltpu.VMEM((peers, 8, half), BF16),
            pltpu.VMEM((SHARES, CHUNKS * rows, share), BF16),
            pltpu.VMEM((ny - 1, CHUNKS * rows, out_width), BF16),
            pltpu.VMEM((ny - 1, CHUNKS * rows, out_width), BF16),
            pltpu.VMEM((2, peers, 8, 128), BF16),
            pltpu.VMEM((2, peers, 8, 128), BF16),
            dma((3,)),
            dma((3,)),
            dma((3,)),
            dma,
            dma((CHUNKS,)),
            dma,
            dma((3, 2)),
            dma,
            dma((ny - 1, 2)),
            dma((3,)),
            dma((2, 3)),
        ],
        compiler_params=pltpu.CompilerParams(collective_id=0, has_side_effects=True),
    )(
        tokens,
        norm_gain.reshape(1, width),
        routing.T,
        route_weight.T,
        w_gate[0].T,
        w_up[0].T,
        w_down.reshape(depth, width),
    )


def solution(mesh):
    placed = (
        P("ep", None),
        P(),
        P("ep", None),
        P("ep", None),
        P("ep", None, "tp"),
        P("ep", None, "tp"),
        P("ep", "tp", None),
    )
    body = functools.partial(local, mesh.shape["ep"] // NX, mesh.shape["tp"] // 2)
    return jax.shard_map(body, mesh=mesh, in_specs=placed, out_specs=P("ep", "tp"), check_vma=False)
```

time: 60.4 us -> 58.7 us (0.972)
  Pallas kernels: 58.9 us -> 57.2 us
    pallas_call x1, Pallas kernels: 58.9 us -> 57.2 us  [local(): pl.pallas_call(functools.partial(kernel, nz, ny), out_shape=jax.ShapeDtyp...]
where the time goes in v2:
time: 58.7 us; the launch traced here: 58.5 us
  Pallas kernels  57.2 us (97%)
  local copies, waits for them, and re-layouts  1.31 us (2%)
    pallas_call x1, Pallas kernels, local(): pl.pallas_call(functools.partial(kernel, nz, ny), out_shape=jax.ShapeDtyp...  57.2 us
    unnamed x1, local copies, waits for them, and re-layouts  1.31 us

profile of v2, /device:TPU:1, one launch (start us, length us, event | category | flops | bytes accessed | tf_op | source)
XLA Modules:
  0.0 58.5 jit_solution(7280448920166784277)
XLA Ops:
  0.0 57.2 %shard_map.73 = bf16[24,192]{1,0:T(8,128)(2,1)} custom-call(bf16[24,3072]{1,0:T(8,128)(2,1)} %tok_ref.1, f32[1,3072]{1,0:T(1,128)} %bitcast.13, s32[4,24]{1,0:T(4,128)} %bitcast.14, f32[4,24]{1,0:T(4,128)} %bitcast.15, bf16[192,3072]{1,0:T(8,128)(2,1)} %bitcast.10, bf16[192,3072]{1,0:T(8,128)(2,1)} %bitcast.11, bf16[192,3072]{1,0:T(8,128)(2,1)} %bitcast.12), custom_call_target="tpu_custom_call" | custom-call | tf_op jit(solution)/shard_map/pallas_call | solution.py:314
  57.2 1.3 %copy.9 = bf16[24,192]{1,0:T(8,128)(2,1)} copy(bf16[24,192]{1,0:T(8,128)(2,1)} %shard_map.73) | data formatting | bytes 18432

commit v3 on v2

--- a/solution.py
+++ b/solution.py
@@ -23,9 +23,9 @@
 
 
 def kernel(
-    nz, ny, tok_ref, gain_ref, route_ref, rw_ref, wg_ref, wu_ref, wd_ref, out_ref,
-    gw, uw, dw, sbuf, rbuf, xs, ssend, srecv, rsend, rret,
-    w_sem, wp_send, wp_recv, d_send, d_recv, y_send, y_recv, s_send, s_recv, r_send, r_recv,
+    nz, ny, tok_hbm, gain_hbm, route_hbm, rw_hbm, wg_ref, wu_ref, wd_ref, out_ref,
+    tok_ref, gain_ref, route_ref, rw_ref, gw, uw, dw, sbuf, rbuf, xs, own, ssend, srecv, rsend, rret,
+    in_sem, w_sem, wp_send, wp_recv, d_send, d_recv, y_send, y_recv, s_send, s_recv, r_send, r_recv,
 ):
     ep, tp = lax.axis_index("ep"), lax.axis_index("tp")
     z, x = lax.div(ep, NX), lax.rem(ep, NX)
@@ -63,6 +63,14 @@
     for to in sources[::-1] + [dev(0, 0, dy, core) for dy in (2, -2, 1, -1)] + [partner]:
         pl.semaphore_signal(barrier, inc=1, device_id=to, device_id_type=MESH)
 
+    fetches = [
+        pltpu.make_async_copy(src, dst, in_sem.at[n])
+        for n, (src, dst) in enumerate(
+            ((tok_hbm, tok_ref), (gain_hbm, gain_ref), (route_hbm, route_ref), (rw_hbm, rw_ref))
+        )
+    ]
+    for fetch in fetches:
+        fetch.start()
     local = [
         pltpu.make_async_copy(wg_ref, gw.at[0], w_sem.at[0]),
         pltpu.make_async_copy(wu_ref, uw.at[0], w_sem.at[1]),
@@ -75,6 +83,8 @@
             wd_ref.at[:, pl.ds(q * out_width, out_width)], dw.at[0, q], w_sem.at[2]
         ).start()
 
+    for fetch in fetches:
+        fetch.wait()
     values = tok_ref[...].astype(F32)
     scale = lax.rsqrt(jnp.mean(values * values, axis=-1, keepdims=True) + NORM_EPS)
     at = pl.multiple_of(lax.rem(y, SHARES) * share, 128)
@@ -148,10 +158,10 @@
         mixing += [high, (kept - high.astype(F32)).astype(BF16)]
     mixing = jnp.concatenate(mixing, axis=0)
 
-    far_rows, near_rows = (2,), (0, 1)
+    far_rows, near_rows = (1, 2), (0,)
     groups = (far_rows, near_rows)
     spans = [pl.ds(g[0] * rows, len(g) * rows) for g in groups]
-    for k in (0, 2, 1):
+    for k in (2, 1, 0):
         part = rbuf.at[pl.ds(k * per, per)]
         remote(part, part, d_send, d_recv.at[k], partner).wait_recv()
         got = part[...].astype(F32).reshape(per * 8, half).astype(BF16)
@@ -210,22 +220,26 @@
         return part[...].astype(F32)
 
     def first_stage(g, hidden):
-        ship(0, g, term(hidden, 4), ahead2)
-        ship(1, g, term(hidden, 3), ahead)
-        ship(2, g, term(hidden, -3), behind)
-        ship(3, g, term(hidden, 1), ahead)
-        ship(4, g, term(hidden, -1), behind)
-
-    def relay(g, hidden):
-        own, own_s = term(hidden, 2), term(hidden, -2)
-        ship(5, g, own + take(0, g) + take(1, g), ahead2)
-        ship(6, g, own_s + take(2, g), behind2)
+        terms = {steps: term(hidden, steps) for steps in (4, 3, -3)}
+        ship(0, g, terms[4], ahead2)
+        ship(1, g, terms[3], ahead)
+        ship(2, g, terms[-3], behind)
+        terms = {steps: term(hidden, steps) for steps in (1, -1, 2, -2, 0)}
+        ship(3, g, terms[1], ahead)
+        ship(4, g, terms[-1], behind)
+        own[0, spans[g]] = terms[2]
+        own[1, spans[g]] = terms[-2]
+        own[2, spans[g]] = terms[0]
+
+    def relay(g):
+        ship(5, g, own[0, spans[g]] + take(0, g) + take(1, g), ahead2)
+        ship(6, g, own[1, spans[g]] + take(2, g), behind2)
 
     is_0 = core == 0
     lane = 128
 
-    def give_back(g, hidden):
-        total = term(hidden, 0)
+    def give_back(g):
+        total = own[2, spans[g]]
         for slot in (3, 4, 6, 5):
             total = total + take(slot, g)
         total = total.astype(BF16)
@@ -253,14 +267,12 @@
                 def _():
                     rret[1, 0] = same[0]
 
-    hidden_far = hidden_of(0)
-    first_stage(0, hidden_far)
-    hidden_near = hidden_of(1)
-    relay(0, hidden_far)
-    first_stage(1, hidden_near)
-    give_back(0, hidden_far)
-    relay(1, hidden_near)
-    give_back(1, hidden_near)
+    first_stage(0, hidden_of(0))
+    first_stage(1, hidden_of(1))
+    relay(0)
+    give_back(0)
+    relay(1)
+    give_back(1)
 
     for g in range(2):
         begin, count = groups[g][0] * per, len(groups[g]) * per
@@ -314,19 +326,25 @@
     return pl.pallas_call(
         functools.partial(kernel, nz, ny),
         out_shape=jax.ShapeDtypeStruct((toks, width // (2 * ny)), BF16),
-        in_specs=[vmem()] * 4 + [hbm()] * 3,
+        in_specs=[hbm()] * 7,
         out_specs=vmem(),
         scratch_shapes=[
+            pltpu.VMEM((toks, width), BF16),
+            pltpu.VMEM((1, width), F32),
+            pltpu.VMEM(routing.shape[::-1], jnp.int32),
+            pltpu.VMEM(routing.shape[::-1], F32),
             pltpu.VMEM((2, depth, width), BF16),
             pltpu.VMEM((2, depth, width), BF16),
             pltpu.VMEM((2, ny, depth, out_width), BF16),
             pltpu.VMEM((peers, 8, half), BF16),
             pltpu.VMEM((peers, 8, half), BF16),
             pltpu.VMEM((SHARES, CHUNKS * rows, share), BF16),
+            pltpu.VMEM((3, CHUNKS * rows, out_width), F32),
             pltpu.VMEM((ny - 1, CHUNKS * rows, out_width), BF16),
             pltpu.VMEM((ny - 1, CHUNKS * rows, out_width), BF16),
             pltpu.VMEM((2, peers, 8, 128), BF16),
             pltpu.VMEM((2, peers, 8, 128), BF16),
+            dma((4,)),
             dma((3,)),
             dma((3,)),
             dma((3,)),

time: 58.7 us -> 56.2 us (0.957)
  Pallas kernels: 57.2 us -> 54.7 us
    pallas_call x1, Pallas kernels: 57.2 us -> 54.7 us  [local(): pl.pallas_call(functools.partial(kernel, nz, ny), out_shape=jax.ShapeDtyp...]
where the time goes in v3:
time: 56.2 us; the launch traced here: 56 us
  Pallas kernels  54.7 us (97%)
  local copies, waits for them, and re-layouts  1.31 us (2%)
    pallas_call x1, Pallas kernels, local(): pl.pallas_call(functools.partial(kernel, nz, ny), out_shape=jax.ShapeDtyp...  54.7 us
    unnamed x1, local copies, waits for them, and re-layouts  1.31 us

profile of v3, /device:TPU:1, one launch (start us, length us, event | category | flops | bytes accessed | tf_op | source)
XLA Modules:
  0.0 56.0 jit_solution(11355661423364545379)
XLA Ops:
  0.0 54.7 %shard_map.73 = bf16[24,192]{1,0:T(8,128)(2,1)} custom-call(bf16[24,3072]{1,0:T(8,128)(2,1)} %tok_hbm.1, f32[1,3072]{1,0:T(1,128)} %bitcast.13, s32[4,24]{1,0:T(4,128)} %bitcast.14, f32[4,24]{1,0:T(4,128)} %bitcast.15, bf16[192,3072]{1,0:T(8,128)(2,1)} %bitcast.10, bf16[192,3072]{1,0:T(8,128)(2,1)} %bitcast.11, bf16[192,3072]{1,0:T(8,128)(2,1)} %bitcast.12), custom_call_target="tpu_custom_call" | custom-call | tf_op jit(solution)/shard_map/pallas_call | solution.py:326
  54.7 1.3 %copy.9 = bf16[24,192]{1,0:T(8,128)(2,1)} copy(bf16[24,192]{1,0:T(8,128)(2,1)} %shard_map.73) | data formatting | bytes 18432

commit v4 on v3

--- a/solution.py
+++ b/solution.py
@@ -24,7 +24,7 @@
 
 def kernel(
     nz, ny, tok_hbm, gain_hbm, route_hbm, rw_hbm, wg_ref, wu_ref, wd_ref, out_ref,
-    tok_ref, gain_ref, route_ref, rw_ref, gw, uw, dw, sbuf, rbuf, xs, own, ssend, srecv, rsend, rret,
+    tok_ref, gain_ref, route_ref, rw_ref, gw, uw, dw, sbuf, rbuf, xs, acc, own, ssend, srecv, rsend, rret,
     in_sem, w_sem, wp_send, wp_recv, d_send, d_recv, y_send, y_recv, s_send, s_recv, r_send, r_recv,
 ):
     ep, tp = lax.axis_index("ep"), lax.axis_index("tp")
@@ -40,12 +40,12 @@
 
     def dev(dz, dx, dy, at):
         return (
-            lax.rem(z + dz + nz, nz) * NX + lax.rem(x + dx + NX, NX),
+            lax.rem(z + dz + 2 * nz, nz) * NX + lax.rem(x + dx + NX, NX),
             lax.rem(y + dy + ny, ny) * 2 + at,
         )
 
-    def far(i):
-        return (i + 1) // 2 if i % 2 else (nz - i // 2) % nz
+    def offset(j, sender):
+        return nz // 4 + sender * (nz // 2) + j // NX, (j + 1) % NX
 
     def remote(src, dst, send, recv, to):
         return pltpu.make_async_remote_copy(
@@ -54,13 +54,16 @@
 
     partner = dev(0, 0, 0, other)
     def source(j, at):
-        return dev(-far(j // 2), -(2 * (j % 2) + other), 0, at)
+        dz, dx = offset(j, other)
+        return dev(-dz, -dx, 0, at)
 
     sources = [source(j, other) for j in range(peers)]
-    targets = [dev(far(j // 2), 2 * (j % 2) + core, 0, other) for j in range(peers)]
+    targets = [dev(*offset(j, core), 0, other) for j in range(peers)]
+    own_slot = peers // 2 + NX - 1
+    chunk_order = (1, 2, 0)
 
     barrier = pltpu.get_barrier_semaphore()
-    for to in sources[::-1] + [dev(0, 0, dy, core) for dy in (2, -2, 1, -1)] + [partner]:
+    for to in sources + [dev(0, 0, dy, core) for dy in (2, -2, 1, -1)] + [partner]:
         pl.semaphore_signal(barrier, inc=1, device_id=to, device_id_type=MESH)
 
     fetches = [
@@ -98,13 +101,12 @@
         0.0,
     ).astype(BF16)
 
-    def placed(parity):
+    def placed(sender):
         row = lax.broadcasted_iota(jnp.int32, (peers * 8, 1), 0)
-        order = row >> 4
-        dz = jnp.where((order & 1) == 1, (order + 1) >> 1, jnp.where(order == 0, 0, nz - (order >> 1)))
-        ez = z + dz
+        ez = z + nz // 4 + sender * (nz // 2) + (row >> 5)
         ez = jnp.where(ez >= nz, ez - nz, ez)
-        expert = ez * NX + ((x + 2 * ((row >> 3) & 1) + parity) & (NX - 1))
+        ez = jnp.where(ez >= nz, ez - nz, ez)
+        expert = ez * NX + ((x + (row >> 3) + 1) & (NX - 1))
         hit = jnp.zeros((peers * 8, toks), F32)
         weight = jnp.zeros((peers * 8, toks), F32)
         for k in range(routes.shape[0]):
@@ -122,7 +124,7 @@
     sbuf[...] = sending.reshape(peers, 8, half).astype(BF16)
 
     pl.semaphore_wait(barrier, peers + 5)
-    for j in reversed(range(peers)):
+    for j in [k * per + n for k in chunk_order for n in range(per)]:
         remote(sbuf.at[j], rbuf.at[j], d_send, d_recv.at[j // per], targets[j]).start()
 
     for copy in local:
@@ -158,17 +160,14 @@
         mixing += [high, (kept - high.astype(F32)).astype(BF16)]
     mixing = jnp.concatenate(mixing, axis=0)
 
-    far_rows, near_rows = (1, 2), (0,)
-    groups = (far_rows, near_rows)
-    spans = [pl.ds(g[0] * rows, len(g) * rows) for g in groups]
-    for k in (2, 1, 0):
+    spans = [pl.ds(k * rows, rows) for k in chunk_order]
+    for g, k in enumerate(chunk_order):
         part = rbuf.at[pl.ds(k * per, per)]
         remote(part, part, d_send, d_recv.at[k], partner).wait_recv()
         got = part[...].astype(F32).reshape(per * 8, half).astype(BF16)
         span = pl.ds(k * rows, rows)
         xs[0, span, :half] = dot(first_c, got).astype(BF16)
         xs[0, span, half:] = dot(second_c, got).astype(BF16)
-        g = 0 if k in far_rows else 1
         whole = xs.at[0, span]
         left, right = xs.at[0, span, pl.ds(0, half)], xs.at[0, span, pl.ds(half, half)]
         remote(left, xs.at[3, span, pl.ds(0, half)], y_send, y_recv.at[2, g], dev(0, 0, 2, core)).start()
@@ -179,20 +178,23 @@
     for push in pushes:
         push.wait_recv()
 
+    def products(block, dy):
+        span = pl.ds(pl.multiple_of(lax.rem(y + dy + SHARES, SHARES) * share, 128), share)
+        return [
+            lax.dot_general(block, w[side, :, span], (((1,), (1,)), ((), ())), preferred_element_type=F32)
+            for side in range(2)
+            for w in (gw, uw)
+        ]
+
+    for n, product in enumerate(products(xs[0], 0)):
+        acc[n] = product
+
     def hidden_of(g):
-        sums = None
-        for n, dy in enumerate((0, -1, 1, 2)):
-            if n:
-                part = xs.at[n, spans[g]]
-                remote(part, part, y_send, y_recv.at[n - 1, g], partner).wait_recv()
-            block = xs[n, spans[g]]
-            span = pl.ds(pl.multiple_of(lax.rem(y + dy + SHARES, SHARES) * share, 128), share)
-            terms = [
-                lax.dot_general(block, w[side, :, span], (((1,), (1,)), ((), ())), preferred_element_type=F32)
-                for side in range(2)
-                for w in (gw, uw)
-            ]
-            sums = terms if sums is None else [a + b for a, b in zip(sums, terms)]
+        sums = [acc[n, spans[g]] for n in range(4)]
+        for n, dy in ((1, -1), (2, 1), (3, 2)):
+            part = xs.at[n, spans[g]]
+            remote(part, part, y_send, y_recv.at[n - 1, g], partner).wait_recv()
+            sums = [a + b for a, b in zip(sums, products(part[...], dy))]
         hidden = []
         for side in range(2):
             gated = jnp.minimum(sums[2 * side], CLAMP_LIMIT)
@@ -237,54 +239,53 @@
 
     is_0 = core == 0
     lane = 128
+    own_chip = remote(
+        rsend.at[0, own_slot], rret.at[core, own_slot], r_send.at[3], r_recv.at[0, CHUNKS], source(own_slot, core)
+    )
 
     def give_back(g):
         total = own[2, spans[g]]
         for slot in (3, 4, 6, 5):
             total = total + take(slot, g)
         total = total.astype(BF16)
-        for k in reversed(groups[g]):
-            at = (k - groups[g][0]) * rows
-            piece = total[at : at + rows]
-            ends, middle = dot(first_e, piece), dot(second_e, piece[:, lane : 2 * lane])
-            spread_0, spread_1 = ends[:, :lane] + middle, ends[:, 2 * lane :] + middle
-            span = pl.ds(k * per, per)
-            same = jnp.where(is_0, spread_0, spread_1).reshape(per, 8, lane).astype(BF16)
-            cross = jnp.where(is_0, spread_1, spread_0).reshape(per, 8, lane).astype(BF16)
-            rsend[0, span] = same
-            rsend[1, span] = cross
-            for j in reversed(range(k * per, (k + 1) * per)):
-                remote(rsend.at[1, j], rret.at[core, j], r_send.at[1], r_recv.at[1, g], source(j, other)).start()
-                if j:
-                    remote(rsend.at[0, j], rret.at[core, j], r_send.at[0], r_recv.at[0, g], source(j, core)).start()
-                    continue
-
-                @pl.when(is_0)
-                def _():
-                    remote(rsend.at[0, 0], rret.at[core, 0], r_send.at[2], r_recv.at[0, 2], source(0, core)).start()
-
-                @pl.when(core == 1)
-                def _():
-                    rret[1, 0] = same[0]
-
-    first_stage(0, hidden_of(0))
-    first_stage(1, hidden_of(1))
-    relay(0)
-    give_back(0)
-    relay(1)
-    give_back(1)
-
-    for g in range(2):
-        begin, count = groups[g][0] * per, len(groups[g]) * per
-        crossed = rret.at[other, pl.ds(begin, count)]
+        ends, middle = dot(first_e, total), dot(second_e, total[:, lane : 2 * lane])
+        spread_0, spread_1 = ends[:, :lane] + middle, ends[:, 2 * lane :] + middle
+        first_slot = chunk_order[g] * per
+        span = pl.ds(first_slot, per)
+        same = jnp.where(is_0, spread_0, spread_1).reshape(per, 8, lane).astype(BF16)
+        cross = jnp.where(is_0, spread_1, spread_0).reshape(per, 8, lane).astype(BF16)
+        rsend[0, span] = same
+        rsend[1, span] = cross
+        for j in range(first_slot, first_slot + per):
+            remote(rsend.at[1, j], rret.at[core, j], r_send.at[1], r_recv.at[1, g], source(j, other)).start()
+            if j != own_slot:
+                to, half_send = source(j, core), r_send.at[0 if j < own_slot else 2]
+                remote(rsend.at[0, j], rret.at[core, j], half_send, r_recv.at[0, g], to).start()
+                continue
+
+            @pl.when(core == 1)
+            def _():
+                own_chip.start()
+
+            @pl.when(is_0)
+            def _():
+                rret[0, own_slot] = same[own_slot - first_slot]
+
+    for g in range(CHUNKS):
+        first_stage(g, hidden_of(g))
+    for g in range(CHUNKS):
+        relay(g)
+    for g in range(CHUNKS):
+        give_back(g)
+
+    for g, k in enumerate(chunk_order):
+        crossed = rret.at[other, pl.ds(k * per, per)]
         remote(crossed, crossed, d_send, r_recv.at[1, g], partner).wait_recv()
-        skipped = 0 if begin else 1
-        stayed = rret.at[core, pl.ds(begin + skipped, count - skipped)]
+        count = per - 1 if own_slot // per == k else per
+        stayed = rret.at[core, pl.ds(k * per, count)]
         remote(stayed, stayed, d_send, r_recv.at[0, g], partner).wait_recv()
 
-    own_chip = remote(rsend.at[0, 0], rret.at[core, 0], r_send.at[2], r_recv.at[0, 2], partner)
-
-    @pl.when(is_0)
+    @pl.when(core == 1)
     def _():
         own_chip.wait_recv()
 
@@ -303,10 +304,11 @@
     remote(others, others, y_send, d_recv.at[0], partner).wait_send()
     remote(ssend, srecv, s_send, d_recv.at[0], partner).wait_send()
     remote(rsend.at[1], rret.at[0], r_send.at[1], d_recv.at[0], partner).wait_send()
-    stayed = rsend.at[0, pl.ds(1, peers - 1)]
-    remote(stayed, stayed, r_send.at[0], d_recv.at[0], partner).wait_send()
-
-    @pl.when(is_0)
+    for n, begin, count in ((0, 0, own_slot), (2, own_slot + 1, peers - 1 - own_slot)):
+        stayed = rsend.at[0, pl.ds(begin, count)]
+        remote(stayed, stayed, r_send.at[n], d_recv.at[0], partner).wait_send()
+
+    @pl.when(core == 1)
     def _():
         own_chip.wait_send()
 
@@ -339,6 +341,7 @@
             pltpu.VMEM((peers, 8, half), BF16),
             pltpu.VMEM((peers, 8, half), BF16),
             pltpu.VMEM((SHARES, CHUNKS * rows, share), BF16),
+            pltpu.VMEM((4, CHUNKS * rows, depth), F32),
             pltpu.VMEM((3, CHUNKS * rows, out_width), F32),
             pltpu.VMEM((ny - 1, CHUNKS * rows, out_width), BF16),
             pltpu.VMEM((ny - 1, CHUNKS * rows, out_width), BF16),
@@ -351,11 +354,11 @@
             dma,
             dma((CHUNKS,)),
             dma,
-            dma((3, 2)),
+            dma((3, CHUNKS)),
             dma,
-            dma((ny - 1, 2)),
-            dma((3,)),
-            dma((2, 3)),
+            dma((ny - 1, CHUNKS)),
+            dma((4,)),
+            dma((2, CHUNKS + 1)),
         ],
         compiler_params=pltpu.CompilerParams(collective_id=0, has_side_effects=True),
     )(

time: 56.2 us -> 52.5 us (0.934)
  Pallas kernels: 54.7 us -> 51 us
    pallas_call x1, Pallas kernels: 54.7 us -> 51 us  [local(): pl.pallas_call(functools.partial(kernel, nz, ny), out_shape=jax.ShapeDtyp...]
where the time goes in v4:
time: 52.5 us; the launch traced here: 52.3 us
  Pallas kernels  51 us (97%)
  local copies, waits for them, and re-layouts  1.31 us (2%)
    pallas_call x1, Pallas kernels, local(): pl.pallas_call(functools.partial(kernel, nz, ny), out_shape=jax.ShapeDtyp...  51 us
    unnamed x1, local copies, waits for them, and re-layouts  1.31 us

profile of v4, /device:TPU:1, one launch (start us, length us, event | category | flops | bytes accessed | tf_op | source)
XLA Modules:
  0.0 52.3 jit_solution(11873523931609506461)
XLA Ops:
  0.0 51.0 %shard_map.73 = bf16[24,192]{1,0:T(8,128)(2,1)} custom-call(bf16[24,3072]{1,0:T(8,128)(2,1)} %tok_hbm.1, f32[1,3072]{1,0:T(1,128)} %bitcast.13, s32[4,24]{1,0:T(4,128)} %bitcast.14, f32[4,24]{1,0:T(4,128)} %bitcast.15, bf16[192,3072]{1,0:T(8,128)(2,1)} %bitcast.10, bf16[192,3072]{1,0:T(8,128)(2,1)} %bitcast.11, bf16[192,3072]{1,0:T(8,128)(2,1)} %bitcast.12), custom_call_target="tpu_custom_call" | custom-call | tf_op jit(solution)/shard_map/pallas_call | solution.py:328
  51.0 1.3 %copy.9 = bf16[24,192]{1,0:T(8,128)(2,1)} copy(bf16[24,192]{1,0:T(8,128)(2,1)} %shard_map.73) | data formatting | bytes 18432

commit v5 on v4

--- a/solution.py
+++ b/solution.py
@@ -24,17 +24,17 @@
 
 def kernel(
     nz, ny, tok_hbm, gain_hbm, route_hbm, rw_hbm, wg_ref, wu_ref, wd_ref, out_ref,
-    tok_ref, gain_ref, route_ref, rw_ref, gw, uw, dw, sbuf, rbuf, xs, acc, own, ssend, srecv, rsend, rret,
+    tok_ref, gain_ref, route_ref, rw_ref, guw, dw, packed, spilled, gathered, sbuf, rbuf, xs, acc, own, ssend, srecv, rsend, rret,
     in_sem, w_sem, wp_send, wp_recv, d_send, d_recv, y_send, y_recv, s_send, s_recv, r_send, r_recv,
 ):
     ep, tp = lax.axis_index("ep"), lax.axis_index("tp")
     z, x = lax.div(ep, NX), lax.rem(ep, NX)
     y, core = lax.div(tp, 2), lax.rem(tp, 2)
     other = 1 - core
-    toks = tok_ref.shape[0]
+    toks, depth = tok_ref.shape[0], wd_ref.shape[0]
     peers = sbuf.shape[0]
     per = peers // CHUNKS
-    half = sbuf.shape[2]
+    half = xs.shape[2] // 2
     share = 2 * half
     lanes = out_ref.shape[1]
 
@@ -75,8 +75,8 @@
     for fetch in fetches:
         fetch.start()
     local = [
-        pltpu.make_async_copy(wg_ref, gw.at[0], w_sem.at[0]),
-        pltpu.make_async_copy(wu_ref, uw.at[0], w_sem.at[1]),
+        pltpu.make_async_copy(wg_ref, guw.at[0], w_sem.at[0]),
+        pltpu.make_async_copy(wu_ref, guw.at[2], w_sem.at[1]),
     ]
     for copy in local:
         copy.start()
@@ -101,27 +101,32 @@
         0.0,
     ).astype(BF16)
 
-    def placed(sender):
-        row = lax.broadcasted_iota(jnp.int32, (peers * 8, 1), 0)
-        ez = z + nz // 4 + sender * (nz // 2) + (row >> 5)
+    def named(sender, peer):
+        ez = z + nz // 4 + sender * (nz // 2) + (peer >> 2)
         ez = jnp.where(ez >= nz, ez - nz, ez)
         ez = jnp.where(ez >= nz, ez - nz, ez)
-        expert = ez * NX + ((x + (row >> 3) + 1) & (NX - 1))
-        hit = jnp.zeros((peers * 8, toks), F32)
-        weight = jnp.zeros((peers * 8, toks), F32)
+        expert = ez * NX + ((x + peer + 1) & (NX - 1))
+        hit = jnp.zeros((peer.shape[0], toks), F32)
+        weight = jnp.zeros((peer.shape[0], toks), F32)
         for k in range(routes.shape[0]):
             same = routes[k : k + 1] == expert
             hit = hit + jnp.where(same, 1.0, 0.0)
             weight = weight + jnp.where(same, weights[k : k + 1], 0.0)
-        before = dot(hit.astype(BF16), earlier)
-        here = jnp.where(before == (row & 3).astype(F32), hit, 0.0)
-        return here, weight, (row >> 2) & 1
-
-    here, _, in_half = placed(core)
-    here_0 = jnp.where(in_half == 0, here, 0.0)
-    here_1 = here - here_0
-    sending = dot(here_0.astype(BF16), normal[:, :half]) + dot(here_1.astype(BF16), normal[:, half:])
-    sbuf[...] = sending.reshape(peers, 8, half).astype(BF16)
+        return hit, weight, dot(hit.astype(BF16), earlier)
+
+    row = lax.broadcasted_iota(jnp.int32, (peers * 2, 1), 0)
+    hit, _, before = named(core, row >> 1)
+
+    def pick(at, place):
+        return jnp.where(((row & 1) == at) & (before == place), hit, 0.0).astype(BF16)
+
+    first_half, second_half = normal[:, :half], normal[:, half:]
+    upper_0, upper_1, lower_1, lower_2 = pick(0, 0.0), pick(0, 1.0), pick(1, 1.0), pick(1, 2.0)
+    packed[:, pl.ds(0, half)] = dot(upper_0, first_half) + dot(lower_1, second_half)
+    packed[:, pl.ds(half, half)] = dot(upper_0, second_half) + dot(lower_2, first_half)
+    packed[:, pl.ds(share, half)] = dot(upper_1, first_half) + dot(lower_2, second_half)
+    for j in range(peers):
+        sbuf[j] = packed[pl.ds(2 * j, 2)].astype(BF16)
 
     pl.semaphore_wait(barrier, peers + 5)
     for j in [k * per + n for k in chunk_order for n in range(per)]:
@@ -131,43 +136,51 @@
         copy.wait()
     pltpu.make_async_copy(dw.at[0], dw.at[0], w_sem.at[2]).wait()
     pushes = [
-        remote(buf.at[0], buf.at[1], wp_send.at[n], wp_recv.at[n], partner)
-        for n, buf in enumerate((gw, uw, dw))
+        remote(src, dst, wp_send.at[n], wp_recv.at[n], partner)
+        for n, (src, dst) in enumerate(
+            ((guw.at[0], guw.at[1]), (guw.at[2], guw.at[3]), (dw.at[0], dw.at[1]))
+        )
     ]
     for push in pushes:
         push.start()
 
     rows = per * 3
-    compact_row = lax.broadcasted_iota(jnp.int32, (rows, per * 8), 0)
-    compact_col = lax.broadcasted_iota(jnp.int32, (rows, per * 8), 1)
-    third = (compact_row * 11) >> 5
-    meets = ((compact_col >> 3) == third) & ((compact_col & 3) == compact_row - 3 * third)
-    first = jnp.where(meets & ((compact_col & 4) == 0), 1.0, 0.0)
-    second = jnp.where(meets & ((compact_col & 4) == 4), 1.0, 0.0)
-    first_c, second_c = first.astype(BF16), second.astype(BF16)
-    first_e, second_e = first.T.astype(BF16), second.T.astype(BF16)
-
-    summed = []
-    for sender in range(2):
-        here, weight, _ = placed(1 - sender)
-        summed.append(here * weight)
-    exact = jnp.concatenate(summed, axis=0).T
-    lane_half = (lax.broadcasted_iota(jnp.int32, exact.shape, 1) >> 2) & 1
+    to_row = lax.broadcasted_iota(jnp.int32, (rows, per * 6), 0)
+    from_row = lax.broadcasted_iota(jnp.int32, (rows, per * 6), 1)
+    third, block = (to_row * 11) >> 5, from_row >> 4
+    meets = (((from_row & 15) >> 1) == third) & (block == to_row - 3 * third)
+    first_c = jnp.where(meets & ((from_row & 1) == (block >> 1)), 1.0, 0.0).astype(BF16)
+    second_c = jnp.where(meets & ((from_row & 1) == ((block + 1) >> 1)), 1.0, 0.0).astype(BF16)
+    to_row = lax.broadcasted_iota(jnp.int32, (per * 6, rows), 0)
+    from_row = lax.broadcasted_iota(jnp.int32, (per * 6, rows), 1)
+    meets = from_row == 3 * ((to_row & 15) >> 1) + (to_row >> 4)
+    first_e = jnp.where(meets & ((to_row & 1) == 0), 1.0, 0.0).astype(BF16)
+    second_e = jnp.where(meets & ((to_row & 1) == 1), 1.0, 0.0).astype(BF16)
+
+    row = lax.broadcasted_iota(jnp.int32, (peers * 12, 1), 0)
+    place = jnp.where(row >= peers * 4, 1, 0) + jnp.where(row >= peers * 8, 1, 0)
+    row = row - place * (peers * 4)
+    holder = jnp.where(row >= peers * 2, 1, 0)
+    hit, weight, before = named(1 - holder, (row - holder * (peers * 2)) >> 1)
+    exact = jnp.where(before == place.astype(F32), hit * weight, 0.0).T
+    lane_part = lax.broadcasted_iota(jnp.int32, exact.shape, 1) & 1
     mixing = []
     for part in range(2):
-        kept = jnp.where(lane_half == part, exact, 0.0)
+        kept = jnp.where(lane_part == part, exact, 0.0)
         high = kept.astype(BF16)
         mixing += [high, (kept - high.astype(F32)).astype(BF16)]
     mixing = jnp.concatenate(mixing, axis=0)
 
-    spans = [pl.ds(k * rows, rows) for k in chunk_order]
+    spans = [pl.ds(g * rows, rows) for g in range(CHUNKS)]
     for g, k in enumerate(chunk_order):
         part = rbuf.at[pl.ds(k * per, per)]
         remote(part, part, d_send, d_recv.at[k], partner).wait_recv()
-        got = part[...].astype(F32).reshape(per * 8, half).astype(BF16)
-        span = pl.ds(k * rows, rows)
-        xs[0, span, :half] = dot(first_c, got).astype(BF16)
-        xs[0, span, half:] = dot(second_c, got).astype(BF16)
+        for n in range(per):
+            packed[pl.ds(2 * n, 2)] = rbuf[k * per + n].astype(F32)
+        blocks = [packed[pl.ds(0, 2 * per), pl.ds(n * half, half)].astype(BF16) for n in range(3)]
+        span = spans[g]
+        xs[0, span, :half] = dot(first_c, jnp.concatenate([blocks[0], blocks[2], blocks[1]], axis=0)).astype(BF16)
+        xs[0, span, half:] = dot(second_c, jnp.concatenate([blocks[1], blocks[0], blocks[2]], axis=0)).astype(BF16)
         whole = xs.at[0, span]
         left, right = xs.at[0, span, pl.ds(0, half)], xs.at[0, span, pl.ds(half, half)]
         remote(left, xs.at[3, span, pl.ds(0, half)], y_send, y_recv.at[2, g], dev(0, 0, 2, core)).start()
@@ -180,38 +193,40 @@
 
     def products(block, dy):
         span = pl.ds(pl.multiple_of(lax.rem(y + dy + SHARES, SHARES) * share, 128), share)
-        return [
-            lax.dot_general(block, w[side, :, span], (((1,), (1,)), ((), ())), preferred_element_type=F32)
-            for side in range(2)
-            for w in (gw, uw)
-        ]
-
-    for n, product in enumerate(products(xs[0], 0)):
-        acc[n] = product
-
-    def hidden_of(g):
-        sums = [acc[n, spans[g]] for n in range(4)]
+        both = guw[:, :, span].reshape(4 * depth, share)
+        return lax.dot_general(block, both, (((1,), (1,)), ((), ())), preferred_element_type=F32)
+
+    acc[...] = products(xs[0], 0)
+
+    def hidden_of(gs):
+        span = pl.ds(gs[0] * rows, len(gs) * rows)
+        sums = acc[span]
         for n, dy in ((1, -1), (2, 1), (3, 2)):
-            part = xs.at[n, spans[g]]
-            remote(part, part, y_send, y_recv.at[n - 1, g], partner).wait_recv()
-            sums = [a + b for a, b in zip(sums, products(part[...], dy))]
-        hidden = []
-        for side in range(2):
-            gated = jnp.minimum(sums[2 * side], CLAMP_LIMIT)
-            upper = jnp.clip(sums[2 * side + 1], -CLAMP_LIMIT, CLAMP_LIMIT)
-            hidden.append(((upper + 1.0) * gated * jax.nn.sigmoid(SIGMOID_SCALE * gated)).astype(BF16))
-        return hidden
+            for g in gs:
+                part = xs.at[n, spans[g]]
+                remote(part, part, y_send, y_recv.at[n - 1, g], partner).wait_recv()
+            sums = sums + products(xs[n, span], dy)
+        gated = jnp.minimum(sums[:, : 2 * depth], CLAMP_LIMIT)
+        upper = jnp.clip(sums[:, 2 * depth :], -CLAMP_LIMIT, CLAMP_LIMIT)
+        return ((upper + 1.0) * gated * jax.nn.sigmoid(SIGMOID_SCALE * gated)).astype(BF16)
 
     sign = 1 - 2 * core
     ahead, ahead2 = dev(0, 0, sign, core), dev(0, 0, 2 * sign, core)
     behind, behind2 = dev(0, 0, -sign, core), dev(0, 0, -2 * sign, core)
 
-    def term(hidden, steps):
-        to = lax.rem(y + steps * sign + ny, ny)
-        return dot(hidden[0], dw[0, to]) + dot(hidden[1], dw[1, to])
+    def terms(hidden, steps):
+        blocks = []
+        for step in steps:
+            to = lax.rem(y + step * sign + ny, ny)
+            blocks.append(jnp.concatenate([dw[0, to], dw[1, to]], axis=0))
+        out = dot(hidden, jnp.concatenate(blocks, axis=1))
+        return [out[:, n * out_width : (n + 1) * out_width] for n in range(len(steps))]
 
     def ship(slot, g, value, to):
         ssend[slot, spans[g]] = value.astype(BF16)
+        launch(slot, g, to)
+
+    def launch(slot, g, to):
         remote(
             ssend.at[slot, spans[g]], srecv.at[slot, spans[g]], s_send, s_recv.at[slot, g], to
         ).start()
@@ -221,17 +236,23 @@
         remote(part, part, s_send, s_recv.at[slot, g], partner).wait_recv()
         return part[...].astype(F32)
 
-    def first_stage(g, hidden):
-        terms = {steps: term(hidden, steps) for steps in (4, 3, -3)}
-        ship(0, g, terms[4], ahead2)
-        ship(1, g, terms[3], ahead)
-        ship(2, g, terms[-3], behind)
-        terms = {steps: term(hidden, steps) for steps in (1, -1, 2, -2, 0)}
-        ship(3, g, terms[1], ahead)
-        ship(4, g, terms[-1], behind)
-        own[0, spans[g]] = terms[2]
-        own[1, spans[g]] = terms[-2]
-        own[2, spans[g]] = terms[0]
+    def first_stage(gs, hidden):
+        to_ship = ((0, 4, ahead2), (1, 3, ahead), (2, -3, behind))
+        out = terms(hidden, [step for _, step, _ in to_ship] + [2])
+        for n, g in enumerate(gs):
+            for (slot, _, to), value in zip(to_ship, out):
+                ship(slot, g, value[n * rows : (n + 1) * rows], to)
+            own[0, spans[g]] = out[3][n * rows : (n + 1) * rows]
+        out = terms(hidden, (-2, 0, 1, -1))
+        for n, g in enumerate(gs):
+            for slot, value in enumerate(out[:2]):
+                own[slot + 1, spans[g]] = value[n * rows : (n + 1) * rows]
+            for slot, value in enumerate(out[2:]):
+                ssend[slot + 3, spans[g]] = value[n * rows : (n + 1) * rows].astype(BF16)
+
+    def neighbours(g):
+        launch(3, g, ahead)
+        launch(4, g, behind)
 
     def relay(g):
         ship(5, g, own[0, spans[g]] + take(0, g) + take(1, g), ahead2)
@@ -249,13 +270,15 @@
             total = total + take(slot, g)
         total = total.astype(BF16)
         ends, middle = dot(first_e, total), dot(second_e, total[:, lane : 2 * lane])
-        spread_0, spread_1 = ends[:, :lane] + middle, ends[:, 2 * lane :] + middle
         first_slot = chunk_order[g] * per
-        span = pl.ds(first_slot, per)
-        same = jnp.where(is_0, spread_0, spread_1).reshape(per, 8, lane).astype(BF16)
-        cross = jnp.where(is_0, spread_1, spread_0).reshape(per, 8, lane).astype(BF16)
-        rsend[0, span] = same
-        rsend[1, span] = cross
+        spreads = []
+        for spread in (ends[:, :lane] + middle, ends[:, 2 * lane :] + middle):
+            spreads.append(jnp.concatenate([spread[n * 2 * per : (n + 1) * 2 * per] for n in range(3)], axis=1))
+        spilled[0] = jnp.where(is_0, spreads[0], spreads[1])
+        spilled[1] = jnp.where(is_0, spreads[1], spreads[0])
+        for n in range(per):
+            rsend[0, first_slot + n] = spilled[0, pl.ds(2 * n, 2)].astype(BF16)
+            rsend[1, first_slot + n] = spilled[1, pl.ds(2 * n, 2)].astype(BF16)
         for j in range(first_slot, first_slot + per):
             remote(rsend.at[1, j], rret.at[core, j], r_send.at[1], r_recv.at[1, g], source(j, other)).start()
             if j != own_slot:
@@ -269,12 +292,16 @@
 
             @pl.when(is_0)
             def _():
-                rret[0, own_slot] = same[own_slot - first_slot]
-
-    for g in range(CHUNKS):
-        first_stage(g, hidden_of(g))
+                rret[0, own_slot] = rsend[0, own_slot]
+
+    for gs in ((0,), (1, 2)):
+        first_stage(gs, hidden_of(gs))
+        if gs == (0,):
+            neighbours(0)
     for g in range(CHUNKS):
         relay(g)
+        if g + 1 < CHUNKS:
+            neighbours(g + 1)
     for g in range(CHUNKS):
         give_back(g)
 
@@ -289,7 +316,11 @@
     def _():
         own_chip.wait_recv()
 
-    back = rret[...].astype(F32).reshape(2 * peers * 8, lane).astype(BF16)
+    for holder in range(2):
+        for j in range(peers):
+            gathered[pl.ds((holder * peers + j) * 2, 2)] = rret[holder, j].astype(F32)
+    back = gathered[...].astype(BF16)
+    back = jnp.concatenate([back[:, n * lane : (n + 1) * lane] for n in range(3)], axis=0)
     mixed = dot(mixing, back)
     ends = mixed[:toks] + mixed[toks : 2 * toks]
     middle = mixed[2 * toks : 3 * toks] + mixed[3 * toks :]
@@ -335,18 +366,20 @@
             pltpu.VMEM((1, width), F32),
             pltpu.VMEM(routing.shape[::-1], jnp.int32),
             pltpu.VMEM(routing.shape[::-1], F32),
-            pltpu.VMEM((2, depth, width), BF16),
-            pltpu.VMEM((2, depth, width), BF16),
+            pltpu.VMEM((4, depth, width), BF16),
             pltpu.VMEM((2, ny, depth, out_width), BF16),
-            pltpu.VMEM((peers, 8, half), BF16),
-            pltpu.VMEM((peers, 8, half), BF16),
+            pltpu.VMEM((peers * 2, 3 * half), F32),
+            pltpu.VMEM((2, per * 2, 384), F32),
+            pltpu.VMEM((peers * 4, 384), F32),
+            pltpu.VMEM((peers, 2, 3 * half), BF16),
+            pltpu.VMEM((peers, 2, 3 * half), BF16),
             pltpu.VMEM((SHARES, CHUNKS * rows, share), BF16),
-            pltpu.VMEM((4, CHUNKS * rows, depth), F32),
+            pltpu.VMEM((CHUNKS * rows, 4 * depth), F32),
             pltpu.VMEM((3, CHUNKS * rows, out_width), F32),
             pltpu.VMEM((ny - 1, CHUNKS * rows, out_width), BF16),
             pltpu.VMEM((ny - 1, CHUNKS * rows, out_width), BF16),
-            pltpu.VMEM((2, peers, 8, 128), BF16),
-            pltpu.VMEM((2, peers, 8, 128), BF16),
+            pltpu.VMEM((2, peers, 2, 384), BF16),
+            pltpu.VMEM((2, peers, 2, 384), BF16),
             dma((4,)),
             dma((3,)),
             dma((3,)),

time: 52.5 us -> 50.9 us (0.970)
  Pallas kernels: 51 us -> 49.4 us
    pallas_call x1, Pallas kernels: 51 us -> 49.4 us  [local(): pl.pallas_call(functools.partial(kernel, nz, ny), out_shape=jax.ShapeDtyp...]
where the time goes in v5:
time: 50.9 us; the launch traced here: 50.7 us
  Pallas kernels  49.4 us (97%)
  local copies, waits for them, and re-layouts  1.31 us (3%)
    pallas_call x1, Pallas kernels, local(): pl.pallas_call(functools.partial(kernel, nz, ny), out_shape=jax.ShapeDtyp...  49.4 us
    unnamed x1, local copies, waits for them, and re-layouts  1.31 us

profile of v5, /device:TPU:1, one launch (start us, length us, event | category | flops | bytes accessed | tf_op | source)
XLA Modules:
  0.0 50.7 jit_solution(16954872969336363711)
XLA Ops:
  0.0 49.4 %shard_map.73 = bf16[24,192]{1,0:T(8,128)(2,1)} custom-call(bf16[24,3072]{1,0:T(8,128)(2,1)} %tok_hbm.1, f32[1,3072]{1,0:T(1,128)} %bitcast.13, s32[4,24]{1,0:T(4,128)} %bitcast.14, f32[4,24]{1,0:T(4,128)} %bitcast.15, bf16[192,3072]{1,0:T(8,128)(2,1)} %bitcast.10, bf16[192,3072]{1,0:T(8,128)(2,1)} %bitcast.11, bf16[192,3072]{1,0:T(8,128)(2,1)} %bitcast.12), custom_call_target="tpu_custom_call" | custom-call | tf_op jit(solution)/shard_map/pallas_call | solution.py:359
  49.4 1.3 %copy.9 = bf16[24,192]{1,0:T(8,128)(2,1)} copy(bf16[24,192]{1,0:T(8,128)(2,1)} %shard_map.73) | data formatting | bytes 18432

commit v6 on v5

--- a/solution.py
+++ b/solution.py
@@ -308,17 +308,18 @@
     for g, k in enumerate(chunk_order):
         crossed = rret.at[other, pl.ds(k * per, per)]
         remote(crossed, crossed, d_send, r_recv.at[1, g], partner).wait_recv()
-        count = per - 1 if own_slot // per == k else per
-        stayed = rret.at[core, pl.ds(k * per, count)]
+        holds_own = own_slot // per == k
+        stayed = rret.at[core, pl.ds(k * per, per - 1 if holds_own else per)]
         remote(stayed, stayed, d_send, r_recv.at[0, g], partner).wait_recv()
-
-    @pl.when(core == 1)
-    def _():
-        own_chip.wait_recv()
-
-    for holder in range(2):
-        for j in range(peers):
-            gathered[pl.ds((holder * peers + j) * 2, 2)] = rret[holder, j].astype(F32)
+        if holds_own:
+
+            @pl.when(core == 1)
+            def _():
+                own_chip.wait_recv()
+
+        for holder in range(2):
+            for j in range(k * per, (k + 1) * per):
+                gathered[pl.ds((holder * peers + j) * 2, 2)] = rret[holder, j].astype(F32)
     back = gathered[...].astype(BF16)
     back = jnp.concatenate([back[:, n * lane : (n + 1) * lane] for n in range(3)], axis=0)
     mixed = dot(mixing, back)

time: 50.9 us -> 50.9 us (level)
  no operation moved by 1% of the time
where the time goes in v6:
time: 50.9 us; the launch traced here: 50.7 us
  Pallas kernels  49.4 us (97%)
  local copies, waits for them, and re-layouts  1.31 us (3%)
    pallas_call x1, Pallas kernels, local(): pl.pallas_call(functools.partial(kernel, nz, ny), out_shape=jax.ShapeDtyp...  49.4 us
    unnamed x1, local copies, waits for them, and re-layouts  1.31 us

profile of v6, /device:TPU:1, one launch (start us, length us, event | category | flops | bytes accessed | tf_op | source)
XLA Modules:
  0.0 50.7 jit_solution(6978669761311311186)
XLA Ops:
  0.0 49.4 %shard_map.73 = bf16[24,192]{1,0:T(8,128)(2,1)} custom-call(bf16[24,3072]{1,0:T(8,128)(2,1)} %tok_hbm.1, f32[1,3072]{1,0:T(1,128)} %bitcast.13, s32[4,24]{1,0:T(4,128)} %bitcast.14, f32[4,24]{1,0:T(4,128)} %bitcast.15, bf16[192,3072]{1,0:T(8,128)(2,1)} %bitcast.10, bf16[192,3072]{1,0:T(8,128)(2,1)} %bitcast.11, bf16[192,3072]{1,0:T(8,128)(2,1)} %bitcast.12), custom_call_target="tpu_custom_call" | custom-call | tf_op jit(solution)/shard_map/pallas_call | solution.py:360
  49.4 1.3 %copy.9 = bf16[24,192]{1,0:T(8,128)(2,1)} copy(bf16[24,192]{1,0:T(8,128)(2,1)} %shard_map.73) | data formatting | bytes 18432
